TPU v7x, 32 devices: a whole 2x2x4 slice. The times are simulated.
32 devices in a mesh: rep: 2 (over x), fs: 8 (over z, y), tp: 2 (over core).
Axes of the slice: x: 2, y: 2, z: 4, core: 2. Of those that a mesh axis runs over, the one named last changes fastest.
Arguments:
- tokens: bfloat16 [16, 192, 2048], P(('rep', 'fs'), 'tp'), may hold values from -6 to 6
- mix_gain: float32 [2048], replicated, may hold values from 0.1 to 1.9
- w_query: float32 [2048, 2048], P('fs', 'tp'), may hold values from -0.125 to 0.125
- w_key: float32 [2048, 2048], P('fs', 'tp'), may hold values from -0.125 to 0.125
- w_value: float32 [2048, 2048], P('fs', 'tp'), may hold values from -0.125 to 0.125
- w_out: float32 [2048, 2048], P('tp', 'fs'), may hold values from -0.125 to 0.125
- scale_query: float32 [2048], P('tp'), may hold values from 0.1 to 1.9
- scale_key: float32 [2048], P('tp'), may hold values from 0.1 to 1.9
- scale_value: float32 [2048], P('tp'), may hold values from 0.1 to 1.9
- scale_out: float32 [2048], replicated, may hold values from 0.1 to 1.9
- decay_rate: float32 [8], P('tp'), may hold values from 0.003 to 0.08
- mlp_gain: float32 [2048], replicated, may hold values from 0.1 to 1.9
- w_gate: float32 [2048, 3072], P('fs', 'tp'), may hold values from -0.125 to 0.125
- w_up: float32 [2048, 3072], P('fs', 'tp'), may hold values from -0.125 to 0.125
- w_down: float32 [3072, 2048], P('tp', 'fs'), may hold values from -0.109375 to 0.109375
- scale_gate: float32 [3072], P('tp'), may hold values from 0.1 to 1.9
- scale_up: float32 [3072], P('tp'), may hold values from 0.1 to 1.9
- scale_down: float32 [2048], replicated, may hold values from 0.1 to 1.9
Outputs:
- layer_out: bfloat16 [16, 192, 2048], P(('rep', 'fs'), 'tp')
All inputs are finite; a program needn't handle non-finite values.
Results may differ from a plain program's by a relative error of at most 0.015.
Values may be sent and summed in bfloat16 or wider, within the bound.
A program may use at most 64 MiB of HBM per device.

v0:
```python
import jax
import jax.numpy as jnp
from jax import lax
from jax.sharding import PartitionSpec as P

HEAD_DIM = 256
BLOCK = 64
EPS = 1e-06
ROPE_BASE = 10000.0


def rms_scale(values, gain):
    values = values.astype(jnp.float32)
    return values * lax.rsqrt(jnp.mean(values * values, axis=-1, keepdims=True) + EPS) * gain


def rotary(values, positions):
    width = values.shape[-1]
    half = width // 2
    inv_freq = 1.0 / ROPE_BASE ** (jnp.arange(0, width, 2, dtype=jnp.float32) / width)
    angles = positions.astype(jnp.float32)[:, None] * inv_freq[None, :]
    cosine = jnp.cos(angles)[:, None, :]
    sine = jnp.sin(angles)[:, None, :]
    first = values[..., :half]
    second = values[..., half:]
    return jnp.concatenate(
        [first * cosine - second * sine, first * sine + second * cosine], axis=-1
    )


def retention(query, keyed, valued, rates):
    length, heads, width = query.shape
    nblocks = length // BLOCK

    def split(values):
        return values.reshape(nblocks, BLOCK, heads, width).transpose(0, 2, 1, 3)

    log_gamma = -rates
    inside = jnp.arange(BLOCK, dtype=jnp.float32)
    distance = inside[:, None] - inside[None, :]
    inner_product = jnp.where(
        distance[None] >= 0.0,
        jnp.exp(log_gamma[:, None, None] * jnp.maximum(distance, 0.0)[None]),
        0.0,
    )
    query_decay = jnp.exp(log_gamma[:, None] * (inside[None, :] + 1.0))
    key_decay_factor = jnp.exp(log_gamma[:, None] * (BLOCK - 1.0 - inside[None, :]))
    block_decay = jnp.exp(log_gamma * BLOCK)

    def advance(state, blocks):
        query_block_tile, key_block_tile, value_block_tile = blocks
        attention_scores = jnp.einsum(
            "frk,fvk->frv", query_block_tile, key_block_tile, preferred_element_type=jnp.float32
        )
        decay_weights = (attention_scores * inner_product).astype(jnp.bfloat16)
        local = jnp.einsum(
            "hnm,hmv->hnv", decay_weights, value_block_tile, preferred_element_type=jnp.float32
        )
        carried = jnp.einsum(
            "hnd,hdv->hnv",
            query_block_tile.astype(jnp.float32) * query_decay[:, :, None],
            state,
            precision=lax.Precision.HIGHEST,
        )
        state_update = jnp.einsum(
            "asf,asp->afp",
            key_block_tile.astype(jnp.float32) * key_decay_factor[:, :, None],
            value_block_tile.astype(jnp.float32),
            precision=lax.Precision.HIGHEST,
        )
        return (state * block_decay[:, None, None] + state_update, local + carried)

    initial = jnp.zeros((heads, width, width), jnp.float32)
    _, outs = lax.scan(advance, initial, (split(query), split(keyed), split(valued)))
    return outs.transpose(0, 2, 1, 3).reshape(length, heads, width)


def per_device(
    tokens,
    mix_gain,
    w_query,
    w_key,
    w_value,
    w_out,
    scale_query,
    scale_key,
    scale_value,
    scale_out,
    decay_rate,
    mlp_gain,
    w_gate,
    w_up,
    w_down,
    scale_gate,
    scale_up,
    scale_down,
):
    own_rows = tokens[0]
    all_rows = lax.all_gather(own_rows, "tp", axis=0, tiled=True)
    gathered = rms_scale(all_rows, mix_gain).astype(jnp.bfloat16)
    length = gathered.shape[0]
    width = w_query.shape[1]
    shards = (
        lax.all_gather(w_query.astype(jnp.bfloat16), "fs", axis=0, tiled=True),
        lax.all_gather(w_key.astype(jnp.bfloat16), "fs", axis=0, tiled=True),
        lax.all_gather(w_value.astype(jnp.bfloat16), "fs", axis=0, tiled=True),
    )
    columns = gathered
    query_raw, key_raw, value_raw = tuple(
        (jnp.dot(columns, shard, preferred_element_type=jnp.float32) for shard in shards)
    )
    positions = jnp.arange(length)
    heads_here = width // HEAD_DIM
    query_rows = rotary(
        (query_raw * scale_query).reshape(length, heads_here, HEAD_DIM), positions
    ).astype(jnp.bfloat16)
    key_rows = rotary(
        (key_raw * scale_key).reshape(length, heads_here, HEAD_DIM), positions
    ).astype(jnp.bfloat16)
    value_rows = (
        (value_raw * scale_value).reshape(length, heads_here, HEAD_DIM).astype(jnp.bfloat16)
    )
    retained = retention(query_rows, key_rows, value_rows, decay_rate)
    attended = rms_scale(retained, 1.0).astype(jnp.bfloat16).reshape(length, width)
    out_whole = lax.all_gather(w_out.astype(jnp.bfloat16), "fs", axis=1, tiled=True)
    picked = attended
    mixed = lax.psum_scatter(
        (jnp.dot(picked, out_whole, preferred_element_type=jnp.float32) * scale_out).astype(
            jnp.bfloat16
        ),
        "tp",
        scatter_dimension=0,
        tiled=True,
    ).astype(jnp.float32)
    hidden_state = (own_rows.astype(jnp.float32) + mixed).astype(jnp.bfloat16)
    mlp_in = rms_scale(hidden_state, mlp_gain).astype(jnp.bfloat16)
    mlp_rows_in = lax.all_gather(mlp_in, "tp", axis=0, tiled=True)
    shards = (
        lax.all_gather(w_gate.astype(jnp.bfloat16), "fs", axis=0, tiled=True),
        lax.all_gather(w_up.astype(jnp.bfloat16), "fs", axis=0, tiled=True),
    )
    columns = mlp_rows_in
    gate_val, up_val = tuple(
        (jnp.dot(columns, shard, preferred_element_type=jnp.float32) for shard in shards)
    )
    down_whole = lax.all_gather(w_down.astype(jnp.bfloat16), "fs", axis=1, tiled=True)
    inner_product = (jax.nn.silu(gate_val * scale_gate) * (up_val * scale_up)).astype(jnp.bfloat16)
    picked = inner_product
    channel = lax.psum_scatter(
        (jnp.dot(picked, down_whole, preferred_element_type=jnp.float32) * scale_down).astype(
            jnp.bfloat16
        ),
        "tp",
        scatter_dimension=0,
        tiled=True,
    ).astype(jnp.float32)
    return (hidden_state.astype(jnp.float32) + channel).astype(jnp.bfloat16)[None]


def solution(mesh):
    in_specs = (
        P(("rep", "fs"), "tp", None),
        P(),
        P("fs", "tp"),
        P("fs", "tp"),
        P("fs", "tp"),
        P("tp", "fs"),
        P("tp"),
        P("tp"),
        P("tp"),
        P(),
        P("tp"),
        P(),
        P("fs", "tp"),
        P("fs", "tp"),
        P("tp", "fs"),
        P("tp"),
        P("tp"),
        P(),
    )
    out_specs = P(("rep", "fs"), "tp", None)
    return jax.shard_map(
        per_device, mesh=mesh, in_specs=in_specs, out_specs=out_specs, check_vma=False
    )
```

profile of v0, /device:TPU:0, one launch (start us, length us, event | category | flops | bytes accessed | tf_op | source)
XLA Modules:
  0.0 641.8 jit_solution(169841490198912978)
XLA Ops:
  6.5 2.2 convert_element_type.108
  8.8 0.9 convert_element_type.113
  9.8 0.4 copy-done.7
  10.1 0.9 convert_element_type.110
  11.1 0.8 convert_element_type.115
  12.2 2.5 all-gather
  14.7 0.2 fusion.52
  14.9 0.4 multiply_cosine_fusion
  15.3 69.7 %all-gather.9.cloned.1.call-done = bf16[2048,1024]{1,0:T(8,128)(2,1)} async-done(((bf16[256,1024]{1,0:T(8,128)(2,1)}), bf16[2048,1024]{1,0:T(8,128)(2,1)}) %all-gather.9.cloned.1.call-update) | async-done | bytes 4194320 | tf_op jit(solution)/shard_map/all_gather | solution.py:105
  85.0 4.1 convolution_multiply_fusion.7
  89.2 1.5 reshape.164
  90.7 67.8 %all-gather.13.cloned.1.call-done = bf16[2048,1024]{1,0:T(8,128)(2,1)} async-done(((bf16[256,1024]{1,0:T(8,128)(2,1)}), bf16[2048,1024]{1,0:T(8,128)(2,1)}) %all-gather.13.cloned.1.call-update) | async-done | bytes 4194320 | tf_op jit(solution)/shard_map/all_gather | solution.py:104
  158.5 4.1 convolution_multiply_fusion.5
  162.6 2.4 reshape.165
  165.1 66.9 %all-gather.11.cloned.1.call-done = bf16[2048,1024]{1,0:T(8,128)(2,1)} async-done(((bf16[256,1024]{1,0:T(8,128)(2,1)}), bf16[2048,1024]{1,0:T(8,128)(2,1)}) %all-gather.11.cloned.1.call-update) | async-done | bytes 4194320 | tf_op jit(solution)/shard_map/all_gather | solution.py:106
  232.0 4.0 fusion.55
  236.0 1.3 convert_element_type.112
  237.3 1.3 fusion.70
  238.9 8.3 %while.15 = (s32[]{:T(128)}, f32[4,256,256]{2,1,0:T(8,128)S(1)}, f32[3,4,64,256]{3,2,1,0:T(8,128)}, f32[4]{0:T(128)S(1)}, bf16[3,4,64,256]{3,2,0,1:T(8,128)(2,1)...) while((s32[]{:T(128)}, f32[4,256,256]{2,1,0:T(8,128)S(1)}, ...), condition=%wide.region_2.3_spmd.clone.clone.clone, body=%wide.region_1.2_spmd.clone.clone.clone.sunk | while | flops 420872704 | bytes 4770468 | solution.py:74
  239.0 0.8 fusion.98
  239.8 1.0 fusion.99
  240.8 0.8 convolution_add_fusion.3
  241.8 0.8 fusion.98
  242.6 1.0 fusion.99
  243.6 0.8 convolution_add_fusion.3
  244.5 0.8 fusion.98
  245.4 1.0 fusion.99
  246.4 0.8 convolution_add_fusion.3
  247.2 1.4 multiply_reduce_fusion
  248.8 0.3 mul.353
  249.2 0.5 copy.43
  249.9 57.2 %all-gather.15.cloned.1.call-done = bf16[1024,2048]{1,0:T(8,128)(2,1)} async-done(((bf16[1024,256]{1,0:T(8,128)(2,1)}), bf16[1024,2048]{1,0:T(8,128)(2,1)}) %all-gather.15.cloned.1.call-update) | async-done | bytes 4194320 | tf_op jit(solution)/shard_map/all_gather | solution.py:125
  307.1 4.2 fusion.49
  311.4 1.0 convert_element_type.121
  312.4 0.6 copy-done.4
  313.0 1.0 convert_element_type.122
  314.1 1.0 convert_element_type.124
  315.2 2.6 reduce-scatter.3.cloned.1.call-done
  317.8 1.2 fusion.56
  319.0 1.2 fusion.58
  320.2 2.5 all_gather.32
  322.8 96.9 %all-gather.17.cloned.1.call-done = bf16[2048,1536]{1,0:T(8,128)(2,1)} async-done(((bf16[256,1536]{1,0:T(8,128)(2,1)}), bf16[2048,1536]{1,0:T(8,128)(2,1)}) %all-gather.17.cloned.1.call-update) | async-done | bytes 6291472 | tf_op jit(solution)/shard_map/all_gather | solution.py:139
  419.7 4.2 convolution_multiply_fusion.2
  423.9 94.9 %all-gather.19.cloned.1.call-done = bf16[2048,1536]{1,0:T(8,128)(2,1)} async-done(((bf16[256,1536]{1,0:T(8,128)(2,1)}), bf16[2048,1536]{1,0:T(8,128)(2,1)}) %all-gather.19.cloned.1.call-update) | async-done | bytes 6291472 | tf_op jit(solution)/shard_map/all_gather | solution.py:140
  518.8 99.7 %all-gather.21.cloned.1.call-done = bf16[1536,2048]{1,0:T(8,128)(2,1)} async-done(((bf16[1536,256]{1,0:T(8,128)(2,1)}), bf16[1536,2048]{1,0:T(8,128)(2,1)}) %all-gather.21.cloned.1.call-update) | async-done | bytes 6291472 | tf_op jit(solution)/shard_map/all_gather | solution.py:146
  618.6 8.3 %fusion.50 = bf16[192,2048]{1,0:T(8,128)(2,1)} fusion(bf16[1536,2048]{1,0:T(8,128)(2,1)} %all-gather.21.cloned.1.call-done, f32[2048]{0:T(1024)S(1)} %copy-done.13, bf16[192,2048]{1,0:T(8,128)(2,1)S(1)} %all_gather.32, bf16[2048,1536]{1,0:T(8,128)(2,1)} %all-gather.19.cloned.1.call-done, f32[192,1536]{1,0:T(8,128)S(1)} %convolution_multiply_fusion.2, ...), kind=kOutput, calls=%fused_computation.51 | convolution fusion | flops 2418769920 | bytes 15349760 | tf_op jit(solution)/shard_map/dot_general | solution.py:150
  626.9 6.5 %reduce-scatter.5.cloned.1.call-done = bf16[96,2048]{1,0:T(8,128)(2,1)} async-done(((bf16[192,2048]{1,0:T(8,128)(2,1)}), bf16[96,2048]{1,0:T(8,128)(2,1)}) %reduce-scatter.5.cloned.1.call-update) | async-done | bytes 393232 | tf_op jit(solution)/shard_map/reduce_scatter | solution.py:149
  633.4 1.9 fusion.63
  (75 shorter events, 1.6 us)
Async XLA Ops:
  6.5 2.3 copy-start.6
  6.5 78.5 %all-gather.9.cloned.1.call-start = ((), (), s32[]{:S(2)}) async-start(), calls=%async_computation.2 | async-start | bytes 4718592 | tf_op jit(solution)/shard_map/all_gather | solution.py:105
  8.7 1.4 copy-start.7
  8.8 149.7 %all-gather.13.cloned.1.call-start = ((), (), s32[]{:S(2)}) async-start(), calls=%async_computation.4 | async-start | bytes 4718592 | tf_op jit(solution)/shard_map/all_gather | solution.py:104
  9.7 1.4 copy-start.8
  9.7 222.3 %all-gather.11.cloned.1.call-start = ((), (), s32[]{:S(2)}) async-start(), calls=%async_computation.3 | async-start | bytes 4718592 | tf_op jit(solution)/shard_map/all_gather | solution.py:106
  11.0 1.1 copy-start
  11.1 296.0 %all-gather.15.cloned.1.call-start = ((), (), s32[]{:S(2)}) async-start(), calls=%async_computation.5 | async-start | bytes 4718592 | tf_op jit(solution)/shard_map/all_gather | solution.py:125
  12.0 2.9 copy-start.18
  12.0 73.0 %copy-start.11 = (f32[2048]{0:T(1024)S(1)}, f32[2048]{0:T(1024)}, u32[]{:S(2)}) copy-start(f32[2048]{0:T(1024)} %param.21) | copy-start | bytes 24580
  12.0 73.0 %copy-start.15 = (f32[1024]{0:T(1024)S(1)}, f32[1024]{0:T(1024)}, u32[]{:S(2)}) copy-start(f32[1024]{0:T(1024)} %param.27) | copy-start | bytes 12292
  12.0 305.8 %reduce-scatter.3.cloned.1.call-start = ((), (), s32[]{:S(2)}) async-start(), calls=%async_computation.6 | async-start | bytes 1179648 | tf_op jit(solution)/shard_map/reduce_scatter | solution.py:127
  89.2 69.3 %copy-start.16 = (f32[1024]{0:T(1024)S(1)}, f32[1024]{0:T(1024)}, u32[]{:S(2)}) copy-start(f32[1024]{0:T(1024)} %param.26) | copy-start | bytes 12292
  162.6 69.3 %copy-start.17 = (f32[1024]{0:T(1024)S(1)}, f32[1024]{0:T(1024)}, u32[]{:S(2)}) copy-start(f32[1024]{0:T(1024)} %param.28) | copy-start | bytes 12292
  247.2 2.0 copy-start.2
  249.2 57.9 %copy-start.9 = (f32[2048]{0:T(1024)S(1)}, f32[2048]{0:T(1024)}, u32[]{:S(2)}) copy-start(f32[2048]{0:T(1024)} %param.29) | copy-start | bytes 24580
  307.1 4.3 copy-start.3
  311.3 1.7 copy-start.4
  311.3 108.4 %all-gather.17.cloned.1.call-start = ((), (), s32[]{:S(2)}) async-start(), calls=%async_computation.7 | async-start | bytes 7077888 | tf_op jit(solution)/shard_map/all_gather | solution.py:139
  312.4 1.7 copy-start.5
  312.4 206.4 %all-gather.19.cloned.1.call-start = ((), (), s32[]{:S(2)}) async-start(), calls=%async_computation.8 | async-start | bytes 7077888 | tf_op jit(solution)/shard_map/all_gather | solution.py:140
  314.0 5.0 copy-start.10
  314.0 304.5 %all-gather.21.cloned.1.call-start = ((), (), s32[]{:S(2)}) async-start(), calls=%async_computation.9 | async-start | bytes 7077888 | tf_op jit(solution)/shard_map/all_gather | solution.py:146
  315.1 104.6 %copy-start.12 = (f32[1536]{0:T(1024)S(1)}, f32[1536]{0:T(1024)}, u32[]{:S(2)}) copy-start(f32[1536]{0:T(1024)} %param.35) | copy-start | bytes 18436
  315.1 318.2 %reduce-scatter.5.cloned.1.call-start = ((), (), s32[]{:S(2)}) async-start(), calls=%async_computation.10 | async-start | bytes 1179648 | tf_op jit(solution)/shard_map/reduce_scatter | solution.py:149
  322.8 295.8 %copy-start.13 = (f32[2048]{0:T(1024)S(1)}, f32[2048]{0:T(1024)}, u32[]{:S(2)}) copy-start(f32[2048]{0:T(1024)} %param.37) | copy-start | bytes 24580
  322.8 295.8 %copy-start.14 = (f32[1536]{0:T(1024)S(1)}, f32[1536]{0:T(1024)}, u32[]{:S(2)}) copy-start(f32[1536]{0:T(1024)} %param.36) | copy-start | bytes 18436
  423.9 209.5 %copy-start.1 = (bf16[96,2048]{1,0:T(8,128)(2,1)S(1)}, bf16[96,2048]{1,0:T(8,128)(2,1)}, u32[]{:S(2)}) copy-start(bf16[96,2048]{1,0:T(8,128)(2,1)} %reduce-scatter.3.cloned.1.call-done) | copy-start | bytes 1179652
Sparse Core Ops, SparseCore 0:
  9.5 75.5 all-gather.8
  87.1 71.3 all-gather.12
  160.6 71.3 all-gather.10
  233.9 73.1 all-gather.14
  311.4 6.3 reduce-scatter.2
  319.8 99.8 all-gather.16
  421.9 96.9 all-gather.18
  520.9 97.6 all-gather.20
  627.0 6.3 reduce-scatter.4
where the time goes:
time: 642 us
  waiting for transfers between devices  563 us (88%)
  matrix products  36.9 us (6%)
  other arithmetic  14.7 us (2%)
  between operations  13.5 us (2%)
  local copies, waits for them, and re-layouts  8.76 us (1%)
    all_gather x1, waiting for transfers between devices, per_device(): lax.all_gather(w_down.astype(jnp.bfloat16), 'fs', axis=1, tiled=True)  99.7 us
    all_gather x1, waiting for transfers between devices, per_device(): lax.all_gather(w_gate.astype(jnp.bfloat16), 'fs', axis=0, tiled=True)  96.9 us
    all_gather x1, waiting for transfers between devices, per_device(): lax.all_gather(w_up.astype(jnp.bfloat16), 'fs', axis=0, tiled=True)  94.9 us
    all_gather x1, waiting for transfers between devices, per_device(): lax.all_gather(w_key.astype(jnp.bfloat16), 'fs', axis=0, tiled=True)  69.7 us
    all_gather x1, waiting for transfers between devices, per_device(): lax.all_gather(w_query.astype(jnp.bfloat16), 'fs', axis=0, tiled=True)  67.8 us
    all_gather x1, waiting for transfers between devices, per_device(): lax.all_gather(w_value.astype(jnp.bfloat16), 'fs', axis=0, tiled=True)  66.9 us
    all_gather x1, waiting for transfers between devices, per_device(): lax.all_gather(w_out.astype(jnp.bfloat16), 'fs', axis=1, tiled=True)  57.2 us
    dot_general x4, matrix products, per_device(): jnp.dot(columns, shard, preferred_element_type=jnp.float32)  16.4 us
  transfers between devices with their start and end apart: 9, of which 9 were waited for; matrix products, arithmetic and copies ran while one was open for 7% of the time, Pallas kernels for 0%

commit v1 on v0

--- a/solution.py
+++ b/solution.py
@@ -143,7 +143,7 @@
     gate_val, up_val = tuple(
         (jnp.dot(columns, shard, preferred_element_type=jnp.float32) for shard in shards)
     )
-    down_whole = lax.all_gather(w_down.astype(jnp.bfloat16), "fs", axis=1, tiled=True)
+    down_whole = jnp.concatenate(lax.all_gather(w_down.astype(jnp.bfloat16), "fs"), axis=1)
     inner_product = (jax.nn.silu(gate_val * scale_gate) * (up_val * scale_up)).astype(jnp.bfloat16)
     picked = inner_product
     channel = lax.psum_scatter(

time: 642 us -> 643 us (level)
  waiting for transfers between devices: 563 us -> 553 us
  local copies, waits for them, and re-layouts: 8.76 us -> 17.5 us
    reshape x0 -> x1, local copies, waits for them, and re-layouts: none -> 8.76 us  [per_device(): jnp.concatenate(lax.all_gather(w_down.astype(jnp.bfloat16), 'fs'), axis=1)]
    all_gather x1, waiting for transfers between devices: 96.9 us -> 90.3 us  [per_device(): lax.all_gather(w_gate.astype(jnp.bfloat16), 'fs', axis=0, tiled=True)]
  transfers between devices with their start and end apart: 9 -> 9, of which waited for: 9 -> 9; matrix products, arithmetic and copies ran while one was open for 7% -> 8% of each run, Pallas kernels for 0% -> 0%
where the time goes in v1:
time: 643 us; the launch traced here: 642 us
  waiting for transfers between devices  553 us (86%)
  matrix products  37.7 us (6%)
  local copies, waits for them, and re-layouts  17.5 us (3%)
  other arithmetic  14.7 us (2%)
  between operations  13.5 us (2%)
    all_gather x1, waiting for transfers between devices, per_device(): lax.all_gather(w_down.astype(jnp.bfloat16), 'fs')  96.9 us
    all_gather x1, waiting for transfers between devices, per_device(): lax.all_gather(w_up.astype(jnp.bfloat16), 'fs', axis=0, tiled=True)  95 us
    all_gather x1, waiting for transfers between devices, per_device(): lax.all_gather(w_gate.astype(jnp.bfloat16), 'fs', axis=0, tiled=True)  90.3 us
    all_gather x1, waiting for transfers between devices, per_device(): lax.all_gather(w_key.astype(jnp.bfloat16), 'fs', axis=0, tiled=True)  69.7 us
    all_gather x1, waiting for transfers between devices, per_device(): lax.all_gather(w_query.astype(jnp.bfloat16), 'fs', axis=0, tiled=True)  67.8 us
    all_gather x1, waiting for transfers between devices, per_device(): lax.all_gather(w_value.astype(jnp.bfloat16), 'fs', axis=0, tiled=True)  66.9 us
    all_gather x1, waiting for transfers between devices, per_device(): lax.all_gather(w_out.astype(jnp.bfloat16), 'fs', axis=1, tiled=True)  57.2 us
    dot_general x4, matrix products, per_device(): jnp.dot(columns, shard, preferred_element_type=jnp.float32)  16.4 us
  transfers between devices with their start and end apart: 9, of which 9 were waited for; matrix products, arithmetic and copies ran while one was open for 8% of the time, Pallas kernels for 0%

profile of v1, /device:TPU:0, one launch (start us, length us, event | category | flops | bytes accessed | tf_op | source)
XLA Modules:
  0.0 641.9 jit_solution(3074652596309704122)
XLA Ops:
  6.5 2.2 convert_element_type.108
  8.8 0.9 convert_element_type.113
  9.8 0.4 copy-done.7
  10.1 0.9 convert_element_type.110
  11.1 0.8 convert_element_type.115
  12.2 2.5 all-gather
  14.9 0.4 multiply_cosine_fusion
  15.3 69.7 %all-gather.10.cloned.1.call-done = bf16[2048,1024]{1,0:T(8,128)(2,1)} async-done(((bf16[256,1024]{1,0:T(8,128)(2,1)}), bf16[2048,1024]{1,0:T(8,128)(2,1)}) %all-gather.10.cloned.1.call-update) | async-done | bytes 4194320 | tf_op jit(solution)/shard_map/all_gather | solution.py:105
  85.0 4.1 convolution_multiply_fusion.7
  89.2 1.5 reshape.170
  90.7 67.8 %all-gather.14.cloned.1.call-done = bf16[2048,1024]{1,0:T(8,128)(2,1)} async-done(((bf16[256,1024]{1,0:T(8,128)(2,1)}), bf16[2048,1024]{1,0:T(8,128)(2,1)}) %all-gather.14.cloned.1.call-update) | async-done | bytes 4194320 | tf_op jit(solution)/shard_map/all_gather | solution.py:104
  158.5 4.1 convolution_multiply_fusion.5
  162.6 2.4 reshape.171
  165.1 66.9 %all-gather.12.cloned.1.call-done = bf16[2048,1024]{1,0:T(8,128)(2,1)} async-done(((bf16[256,1024]{1,0:T(8,128)(2,1)}), bf16[2048,1024]{1,0:T(8,128)(2,1)}) %all-gather.12.cloned.1.call-update) | async-done | bytes 4194320 | tf_op jit(solution)/shard_map/all_gather | solution.py:106
  232.0 4.0 fusion.55
  236.0 1.3 convert_element_type.112
  237.3 1.3 fusion.70
  238.9 8.3 %while.15 = (s32[]{:T(128)}, f32[4,256,256]{2,1,0:T(8,128)S(1)}, f32[3,4,64,256]{3,2,1,0:T(8,128)}, f32[4]{0:T(128)S(1)}, bf16[3,4,64,256]{3,2,0,1:T(8,128)(2,1)...) while((s32[]{:T(128)}, f32[4,256,256]{2,1,0:T(8,128)S(1)}, ...), condition=%wide.region_2.3_spmd.clone.clone.clone, body=%wide.region_1.2_spmd.clone.clone.clone.sunk | while | flops 420872704 | bytes 4770468 | solution.py:74
  239.0 0.8 fusion.98
  239.8 1.0 fusion.99
  240.8 0.8 convolution_add_fusion.3
  241.8 0.8 fusion.98
  242.6 1.0 fusion.99
  243.6 0.8 convolution_add_fusion.3
  244.5 0.8 fusion.98
  245.4 1.0 fusion.99
  246.4 0.8 convolution_add_fusion.3
  247.2 1.4 multiply_reduce_fusion
  248.8 0.3 mul.353
  249.2 0.5 copy.53
  249.9 57.2 %all-gather.16.cloned.1.call-done = bf16[1024,2048]{1,0:T(8,128)(2,1)} async-done(((bf16[1024,256]{1,0:T(8,128)(2,1)}), bf16[1024,2048]{1,0:T(8,128)(2,1)}) %all-gather.16.cloned.1.call-update) | async-done | bytes 4194320 | tf_op jit(solution)/shard_map/all_gather | solution.py:125
  307.1 4.2 fusion.49
  311.4 1.0 convert_element_type.124
  312.5 0.5 copy-done.4
  313.0 1.0 convert_element_type.121
  314.0 1.0 convert_element_type.122
  315.1 2.7 reduce-scatter.3.cloned.1.call-done
  317.8 1.2 fusion.56
  319.0 1.2 fusion.58
  320.2 2.5 all_gather.35
  322.8 96.9 %all-gather.22.cloned.1.call-done = bf16[12288,256]{1,0:T(8,128)(2,1)} async-done(((bf16[1536,256]{1,0:T(8,128)(2,1)}), bf16[12288,256]{1,0:T(8,128)(2,1)}) %all-gather.22.cloned.1.call-update) | async-done | bytes 6291472 | tf_op jit(solution)/shard_map/all_gather | solution.py:146
  419.7 8.8 %copy.56 = bf16[1536,8,256]{0,2,1:T(8,128)(2,1)} copy(bf16[1536,8,256]{2,0,1:T(8,128)(2,1)} %bitcast.94) | data formatting | bytes 12582912 | tf_op jit(solution)/shard_map/reshape | solution.py:146
  428.5 90.3 %all-gather.18.cloned.1.call-done = bf16[2048,1536]{1,0:T(8,128)(2,1)} async-done(((bf16[256,1536]{1,0:T(8,128)(2,1)}), bf16[2048,1536]{1,0:T(8,128)(2,1)}) %all-gather.18.cloned.1.call-update) | async-done | bytes 6291472 | tf_op jit(solution)/shard_map/all_gather | solution.py:139
  518.8 4.2 convolution_multiply_fusion.2
  523.0 95.0 %all-gather.20.cloned.1.call-done = bf16[2048,1536]{1,0:T(8,128)(2,1)} async-done(((bf16[256,1536]{1,0:T(8,128)(2,1)}), bf16[2048,1536]{1,0:T(8,128)(2,1)}) %all-gather.20.cloned.1.call-update) | async-done | bytes 6291472 | tf_op jit(solution)/shard_map/all_gather | solution.py:140
  617.9 9.0 %fusion.50 = bf16[192,2048]{1,0:T(8,128)(2,1)} fusion(bf16[1536,2048]{0,1:T(8,128)(2,1)} %bitcast.95, f32[2048]{0:T(1024)S(1)} %copy-done.13, bf16[192,2048]{1,0:T(8,128)(2,1)S(1)} %all_gather.35, bf16[2048,1536]{1,0:T(8,128)(2,1)} %all-gather.20.cloned.1.call-done, f32[192,1536]{1,0:T(8,128)S(1)} %convolution_multiply_fusion.2, f32[1536]{0:T(1024)S(1)} %copy-done.14), kind=kOutput, calls=%fused_computation.51 | convolution fusion | flops 2418769920 | bytes 15349760 | tf_op jit(solution)/shard_map/dot_general | solution.py:150
  627.0 6.5 %reduce-scatter.5.cloned.1.call-done = bf16[96,2048]{1,0:T(8,128)(2,1)} async-done(((bf16[192,2048]{1,0:T(8,128)(2,1)}), bf16[96,2048]{1,0:T(8,128)(2,1)}) %reduce-scatter.5.cloned.1.call-update) | async-done | bytes 393232 | tf_op jit(solution)/shard_map/reduce_scatter | solution.py:149
  633.5 1.9 fusion.63
  (76 shorter events, 1.9 us)
Async XLA Ops:
  6.5 2.3 copy-start.6
  6.5 78.5 %all-gather.10.cloned.1.call-start = ((), (), s32[]{:S(2)}) async-start(), calls=%async_computation.2 | async-start | bytes 4718592 | tf_op jit(solution)/shard_map/all_gather | solution.py:105
  8.7 1.4 copy-start.7
  8.8 149.7 %all-gather.14.cloned.1.call-start = ((), (), s32[]{:S(2)}) async-start(), calls=%async_computation.4 | async-start | bytes 4718592 | tf_op jit(solution)/shard_map/all_gather | solution.py:104
  9.7 1.4 copy-start.8
  9.7 222.3 %all-gather.12.cloned.1.call-start = ((), (), s32[]{:S(2)}) async-start(), calls=%async_computation.3 | async-start | bytes 4718592 | tf_op jit(solution)/shard_map/all_gather | solution.py:106
  11.0 1.1 copy-start
  11.1 296.0 %all-gather.16.cloned.1.call-start = ((), (), s32[]{:S(2)}) async-start(), calls=%async_computation.5 | async-start | bytes 4718592 | tf_op jit(solution)/shard_map/all_gather | solution.py:125
  12.0 2.9 copy-start.18
  12.0 73.0 %copy-start.11 = (f32[2048]{0:T(1024)S(1)}, f32[2048]{0:T(1024)}, u32[]{:S(2)}) copy-start(f32[2048]{0:T(1024)} %param.21) | copy-start | bytes 24580
  12.0 73.0 %copy-start.15 = (f32[1024]{0:T(1024)S(1)}, f32[1024]{0:T(1024)}, u32[]{:S(2)}) copy-start(f32[1024]{0:T(1024)} %param.27) | copy-start | bytes 12292
  12.0 305.8 %reduce-scatter.3.cloned.1.call-start = ((), (), s32[]{:S(2)}) async-start(), calls=%async_computation.6 | async-start | bytes 1179648 | tf_op jit(solution)/shard_map/reduce_scatter | solution.py:127
  89.2 69.3 %copy-start.16 = (f32[1024]{0:T(1024)S(1)}, f32[1024]{0:T(1024)}, u32[]{:S(2)}) copy-start(f32[1024]{0:T(1024)} %param.26) | copy-start | bytes 12292
  162.6 69.3 %copy-start.17 = (f32[1024]{0:T(1024)S(1)}, f32[1024]{0:T(1024)}, u32[]{:S(2)}) copy-start(f32[1024]{0:T(1024)} %param.28) | copy-start | bytes 12292
  247.2 2.0 copy-start.2
  249.2 57.9 %copy-start.9 = (f32[2048]{0:T(1024)S(1)}, f32[2048]{0:T(1024)}, u32[]{:S(2)}) copy-start(f32[2048]{0:T(1024)} %param.29) | copy-start | bytes 24580
  307.1 4.3 copy-start.3
  311.3 1.7 copy-start.4
  311.3 108.4 %all-gather.22.cloned.1.call-start = ((), (), s32[]{:S(2)}) async-start(), calls=%async_computation.10 | async-start | bytes 7077888 | tf_op jit(solution)/shard_map/all_gather | solution.py:146
  312.4 1.7 copy-start.5
  312.4 206.4 %all-gather.18.cloned.1.call-start = ((), (), s32[]{:S(2)}) async-start(), calls=%async_computation.7 | async-start | bytes 7077888 | tf_op jit(solution)/shard_map/all_gather | solution.py:139
  314.0 5.1 copy-start.10
  314.0 303.9 %all-gather.20.cloned.1.call-start = ((), (), s32[]{:S(2)}) async-start(), calls=%async_computation.8 | async-start | bytes 7077888 | tf_op jit(solution)/shard_map/all_gather | solution.py:140
  315.1 318.4 %reduce-scatter.5.cloned.1.call-start = ((), (), s32[]{:S(2)}) async-start(), calls=%async_computation.9 | async-start | bytes 1179648 | tf_op jit(solution)/shard_map/reduce_scatter | solution.py:149
  419.7 99.1 %copy-start.12 = (f32[1536]{0:T(1024)S(1)}, f32[1536]{0:T(1024)}, u32[]{:S(2)}) copy-start(f32[1536]{0:T(1024)} %param.35) | copy-start | bytes 18436
  428.5 189.5 %copy-start.13 = (f32[2048]{0:T(1024)S(1)}, f32[2048]{0:T(1024)}, u32[]{:S(2)}) copy-start(f32[2048]{0:T(1024)} %param.37) | copy-start | bytes 24580
  428.5 189.5 %copy-start.14 = (f32[1536]{0:T(1024)S(1)}, f32[1536]{0:T(1024)}, u32[]{:S(2)}) copy-start(f32[1536]{0:T(1024)} %param.36) | copy-start | bytes 18436
  617.9 15.6 %copy-start.1 = (bf16[96,2048]{1,0:T(8,128)(2,1)S(1)}, bf16[96,2048]{1,0:T(8,128)(2,1)}, u32[]{:S(2)}) copy-start(bf16[96,2048]{1,0:T(8,128)(2,1)} %reduce-scatter.3.cloned.1.call-done) | copy-start | bytes 1179652
Sparse Core Ops, SparseCore 0:
  9.5 75.5 all-gather.9
  87.1 71.3 all-gather.13
  160.6 71.3 all-gather.11
  233.9 73.1 all-gather.15
  311.4 6.3 reduce-scatter.2
  319.8 99.8 all-gather.21
  421.9 96.8 all-gather.17
  521.0 96.9 all-gather.19
  627.1 6.3 reduce-scatter.4
